TPU v7x, 128 devices: a whole 4x4x4 slice. The times are simulated.
128 devices in a mesh: sp: 16 (over z, x), dp: 8 (over y, core).
Axes of the slice: x: 4, y: 4, z: 4, core: 2. Of those that a mesh axis runs over, the one named last changes fastest.
Arguments:
- hidden_in: bfloat16 [8, 2048, 2048], P('dp', 'sp'), may hold values from -6 to 6
- in_weight: bfloat16 [2048, 512], P(('sp', 'dp')), may hold values from -0.125 to 0.125
- lam_real: float32 [32, 64], replicated, may hold values from -4 to 0, as said below
- lam_imag: float32 [32, 64], replicated, may hold values from 1 to 200
- log_step: float32 [32], replicated, may hold values from -4.61 to -2.3
- b_real: float32 [32, 64, 16], replicated, may hold values from -1 to 1
- b_imag: float32 [32, 64, 16], replicated, may hold values from -1 to 1
- c_real: float32 [32, 16, 64], replicated, may hold values from -0.3 to 0.3
- c_imag: float32 [32, 16, 64], replicated, may hold values from -0.3 to 0.3
- skip_weight: float32 [512], replicated, may hold values from -4 to 4
- lin_weight: bfloat16 [512, 2048], P(None, ('sp', 'dp')), may hold values from -0.25 to 0.25
- gate_weight: bfloat16 [512, 2048], P(None, ('sp', 'dp')), may hold values from -0.25 to 0.25
Outputs:
- mixed: bfloat16 [8, 2048, 2048], P('dp', 'sp')
Inputs may be any that keep to these rules, and one draw needn't show every extreme that they name: `lam_real`: negative in every entry.
All inputs are finite; a program needn't handle non-finite values.
Results may differ from a plain program's by a relative error of at most 0.0047.
The roundings to bfloat16 on the way count: a program that leaves them out, or rounds other values in their place, can miss the bound.
Values may be sent and summed in bfloat16 or wider, within the bound.
A program may use at most 64 MiB of HBM per device.

v0:
```python
import math
import jax
import jax.numpy as jnp
from jax import lax
from jax.sharding import PartitionSpec as P


def rows_first(arrays, axis, dims):
    turned = [jnp.moveaxis(a, dim, 0) for a, dim in zip(arrays, dims)]
    widths = [t[0].size for t in turned]
    both = jnp.concatenate([t.reshape(-1, w) for t, w in zip(turned, widths)], axis=1)
    out = lax.all_gather(both, axis, axis=0, tiled=True)
    tiles = jnp.split(out, [sum(widths[:k]) for k in range(1, len(widths))], axis=1)
    return tuple(
        (
            jnp.moveaxis(b.reshape(-1, *t.shape[1:]), 0, dim)
            for b, t, dim in zip(tiles, turned, dims)
        )
    )


def step_factors(lam_real, lam_imag, log_step, b_real, b_imag):
    step = jnp.exp(log_step)[:, None]
    xpart = lam_real * step
    wpart = lam_imag * step
    decay_re = jnp.exp(xpart) * jnp.cos(wpart)
    decay_im = jnp.exp(xpart) * jnp.sin(wpart)
    numer_re = jnp.expm1(xpart) * jnp.cos(wpart) - 2.0 * jnp.sin(0.5 * wpart) ** 2
    magnitude = lam_real * lam_real + lam_imag * lam_imag
    ratio_re = (numer_re * lam_real + decay_im * lam_imag) / magnitude
    ratio_im = (decay_im * lam_real - numer_re * lam_imag) / magnitude
    bbar_re = ratio_re[..., None] * b_real - ratio_im[..., None] * b_imag
    bbar_im = ratio_re[..., None] * b_imag + ratio_im[..., None] * b_real
    return (decay_re, decay_im, bbar_re, bbar_im)


def combine(left, right):
    lre, lim, lbre, lbim = left
    rre, rim, rbre, rbim = right
    return (
        rre * lre - rim * lim,
        rre * lim + rim * lre,
        rre * lbre - rim * lbim + rbre,
        rre * lbim + rim * lbre + rbim,
    )


def block_scan(piece, factors):
    decay_re, decay_im, bbar_re, bbar_im = factors
    highest = lax.Precision.HIGHEST
    block = piece.shape[0]
    groups_here, states = decay_re.shape
    lanes = groups_here * states
    source = piece.astype(jnp.float32)
    shaped = source.reshape(block, groups_here, source.shape[1] // groups_here)
    drive_re = jnp.einsum("tgh,gph->tgp", shaped, bbar_re, precision=highest).reshape(block, lanes)
    drive_im = jnp.einsum("tgh,gph->tgp", shaped, bbar_im, precision=highest).reshape(block, lanes)
    are = jnp.broadcast_to(decay_re.reshape(lanes), drive_re.shape)
    aim = jnp.broadcast_to(decay_im.reshape(lanes), drive_re.shape)
    return (source, lax.associative_scan(combine, (are, aim, drive_re, drive_im), axis=0))


def run_blocks(sequence, factors, out_re, out_im, direct, start):
    highest = lax.Precision.HIGHEST
    length, width = sequence.shape
    block = math.gcd(length, 512)
    blocks = sequence.reshape(length // block, block, width)
    groups_here, states = factors[0].shape

    def block_step(carry, piece):
        carry_re, carry_im = carry
        source, scanned = block_scan(piece, factors)
        cum_re, cum_im, local_re, local_im = scanned
        state_re = local_re + cum_re * carry_re - cum_im * carry_im
        state_im = local_im + cum_re * carry_im + cum_im * carry_re
        summed = jnp.einsum(
            "tgp,ghp->tgh", state_re.reshape(block, groups_here, states), out_re, precision=highest
        ) - jnp.einsum(
            "tgp,ghp->tgh", state_im.reshape(block, groups_here, states), out_im, precision=highest
        )
        result = jax.nn.gelu(summed.reshape(block, width) + direct * source)
        return ((state_re[-1], state_im[-1]), result.astype(jnp.bfloat16))

    _, results = lax.scan(block_step, start, blocks)
    return results.reshape(length, width)


def by_groups(sequence, lam_real, lam_imag, log_step, b_real, b_imag, c_real, c_imag, skip_weight):
    per_group = b_real.shape[2]
    groups_here = sequence.shape[1] // per_group
    first = lax.axis_index("sp") * groups_here
    pick = lambda table: lax.dynamic_slice_in_dim(table, first, groups_here, 0)
    factors = step_factors(
        pick(lam_real), pick(lam_imag), pick(log_step), pick(b_real), pick(b_imag)
    )
    direct = lax.dynamic_slice_in_dim(skip_weight, first * per_group, groups_here * per_group, 0)
    zeros = jnp.zeros((factors[0].size,), jnp.float32)
    return run_blocks(sequence, factors, pick(c_real), pick(c_imag), direct, (zeros, zeros))


def shards(
    hidden_in,
    in_weight,
    lam_real,
    lam_imag,
    log_step,
    b_real,
    b_imag,
    c_real,
    c_imag,
    skip_weight,
    lin_weight,
    gate_weight,
):
    tok_rows = hidden_in[0]
    whole_in, whole_lin, whole_gate = rows_first(
        (in_weight, lin_weight, gate_weight), ("sp", "dp"), (0, 1, 1)
    )
    inputs = jnp.dot(tok_rows, whole_in, preferred_element_type=jnp.float32).astype(jnp.bfloat16)
    sequence = lax.all_to_all(inputs, "sp", split_axis=1, concat_axis=0, tiled=True)
    mixer_local = by_groups(
        sequence, lam_real, lam_imag, log_step, b_real, b_imag, c_real, c_imag, skip_weight
    )
    mixer_out = lax.all_to_all(mixer_local, "sp", split_axis=0, concat_axis=1, tiled=True)
    linear = jnp.dot(mixer_out, whole_lin, preferred_element_type=jnp.float32)
    gate = jnp.dot(mixer_out, whole_gate, preferred_element_type=jnp.float32)
    mixed = (linear * jax.nn.sigmoid(gate)).astype(jnp.bfloat16)
    return mixed[None]


def solution(mesh):
    placed = (
        P("dp", "sp", None),
        P(("sp", "dp"), None),
        P(),
        P(),
        P(),
        P(),
        P(),
        P(),
        P(),
        P(),
        P(None, ("sp", "dp")),
        P(None, ("sp", "dp")),
    )
    return jax.shard_map(
        shards, mesh=mesh, in_specs=placed, out_specs=P("dp", "sp", None), check_vma=False
    )
```

profile of v0, /device:TPU:0, one launch (start us, length us, event | category | flops | bytes accessed | tf_op | source)
XLA Modules:
  0.0 268.4 jit_solution(9730837093817101557)
XLA Ops:
  6.5 1.4 pad_maximum_fusion.32
  8.0 0.7 dynamic-slice_exponential_fusion
  8.7 0.8 multiply_subtract_fusion.10
  9.8 0.8 add_divide_fusion
  10.8 0.5 multiply_subtract_fusion.17
  11.3 0.7 multiply_add_fusion.9
  12.0 69.2 %all-gather.2.cloned.1.call-done = bf16[2048,1536]{1,0:T(8,128)(2,1)} async-done(((bf16[16,1536]{1,0:T(8,128)(2,1)}), bf16[2048,1536]{1,0:T(8,128)(2,1)}) %all-gather.2.cloned.1.call-update) | async-done | bytes 6291472 | tf_op jit(solution)/shard_map/all_gather | solution.py:12
  81.2 3.0 %fusion.18 = bf16[512,128]{1,0:T(8,128)(2,1)} fusion(bf16[2048,1536]{1,0:T(8,128)(2,1)} %all-gather.2.cloned.1.call-done, bf16[1,128,2048]{2,1,0:T(8,128)(2,1)S(1)} %copy-done), kind=kOutput, calls=%fused_computation.136 | convolution fusion | flops 268500992 | bytes 2752512 | tf_op jit(solution)/shard_map/dot_general | solution.py:119
  84.2 4.4 %all-to-all-start = ((bf16[128,16,32]{0,2,1:T(8,128)(2,1)}), bf16[128,16,32]{0,2,1:T(8,128)(2,1)S(1)}, u32[]{:S(2)}, u32[]{:S(2)}) async-start(bf16[128,16,32]{0,2,1:T(8,128)(2,1)} %bitcast.33), calls=%async_computation | async-start | bytes 262144 | tf_op jit(solution)/shard_map/all_to_all | solution.py:120
  88.8 0.6 slice.1182
  89.5 1.3 dynamic_slice.38
  90.8 0.7 constant_dynamic-slice_fusion.1
  91.5 5.0 %all-to-all-done = bf16[128,16,32]{0,2,1:T(8,128)(2,1)S(1)} async-done(((bf16[128,16,32]{0,2,1:T(8,128)(2,1)}), bf16[128,16,32]{0,2,1:T(8,128)(2,1)S(1)}, u32[]{:S(2)}, u32[]{:S(2)}) %all-to-all-start) | async-done | bytes 131104 | tf_op jit(solution)/shard_map/all_to_all | solution.py:120
  96.7 0.5 broadcast_in_dim.7.clone
  97.8 146.7 %while.18 = (s32[]{:T(128)}, f32[128]{0:T(128)}, f32[128]{0:T(128)}, bf16[4,512,32]{1,2,0:T(8,128)(2,1)S(1)}, bf16[4,512,32]{1,2,0:T(8,128)(2,1)S(1)}, /*index=5...) while((s32[]{:T(128)}, f32[128]{0:T(128)}, ...), condition=%wide.wide.region_1.2_spmd, body=%wide.wide.region_0.1_spmd.sunk | while | flops 53527552 | bytes 26572484 | solution.py:84
  97.8 0.6 pad_add_fusion.9
  98.9 4.5 %slice.1651 = f32[255,128]{0,1:T(8,128)S(1)} slice(f32[512,128]{0,1:T(8,128)S(1)} %bitcast.197), slice={[2:512:2], [0:128:1]} | slice | bytes 261120 | tf_op jit(solution)/shard_map/while/body/eval_jaxpr/slice | solution.py:60
  103.5 4.5 %slice.1598 = f32[256,128]{0,1:T(8,128)S(1)} slice(f32[512,128]{0,1:T(8,128)S(1)} %bitcast.198), slice={[1:512:2], [0:128:1]} | slice | bytes 262144 | tf_op jit(solution)/shard_map/while/body/eval_jaxpr/slice | solution.py:60
  108.0 4.5 %slice.1596 = f32[256,128]{0,1:T(8,128)S(1)} slice(f32[512,128]{0,1:T(8,128)S(1)} %bitcast.199), slice={[0:511:2], [0:128:1]} | slice | bytes 262144 | tf_op jit(solution)/shard_map/while/body/eval_jaxpr/slice | solution.py:60
  113.2 4.5 %slice.1597 = f32[256,128]{0,1:T(8,128)S(1)} slice(f32[512,128]{0,1:T(8,128)S(1)} %bitcast.193), slice={[0:511:2], [0:128:1]} | slice | bytes 262144 | tf_op jit(solution)/shard_map/while/body/eval_jaxpr/slice | solution.py:60
  117.8 4.5 %slice.1595 = f32[256,128]{0,1:T(8,128)S(1)} slice(f32[512,128]{0,1:T(8,128)S(1)} %bitcast.194), slice={[1:512:2], [0:128:1]} | slice | bytes 262144 | tf_op jit(solution)/shard_map/while/body/eval_jaxpr/slice | solution.py:60
  122.3 4.5 %slice.1594 = f32[255,128]{0,1:T(8,128)S(1)} slice(f32[512,128]{0,1:T(8,128)S(1)} %bitcast.195), slice={[2:512:2], [0:128:1]} | slice | bytes 261120 | tf_op jit(solution)/shard_map/while/body/eval_jaxpr/slice | solution.py:60
  130.1 0.6 pad_maximum_fusion.126
  131.0 0.8 multiply_add_fusion.31
  131.8 0.5 slice_bitcast_fusion.6
  132.7 0.5 slice_bitcast_fusion.7
  133.7 0.8 fusion.70
  134.4 0.6 pad_add_fusion.9
  135.6 4.5 %slice.1651 = f32[255,128]{0,1:T(8,128)S(1)} slice(f32[512,128]{0,1:T(8,128)S(1)} %bitcast.197), slice={[2:512:2], [0:128:1]} | slice | bytes 261120 | tf_op jit(solution)/shard_map/while/body/eval_jaxpr/slice | solution.py:60
  140.2 4.5 %slice.1598 = f32[256,128]{0,1:T(8,128)S(1)} slice(f32[512,128]{0,1:T(8,128)S(1)} %bitcast.198), slice={[1:512:2], [0:128:1]} | slice | bytes 262144 | tf_op jit(solution)/shard_map/while/body/eval_jaxpr/slice | solution.py:60
  144.7 4.5 %slice.1596 = f32[256,128]{0,1:T(8,128)S(1)} slice(f32[512,128]{0,1:T(8,128)S(1)} %bitcast.199), slice={[0:511:2], [0:128:1]} | slice | bytes 262144 | tf_op jit(solution)/shard_map/while/body/eval_jaxpr/slice | solution.py:60
  149.9 4.5 %slice.1597 = f32[256,128]{0,1:T(8,128)S(1)} slice(f32[512,128]{0,1:T(8,128)S(1)} %bitcast.193), slice={[0:511:2], [0:128:1]} | slice | bytes 262144 | tf_op jit(solution)/shard_map/while/body/eval_jaxpr/slice | solution.py:60
  154.5 4.5 %slice.1595 = f32[256,128]{0,1:T(8,128)S(1)} slice(f32[512,128]{0,1:T(8,128)S(1)} %bitcast.194), slice={[1:512:2], [0:128:1]} | slice | bytes 262144 | tf_op jit(solution)/shard_map/while/body/eval_jaxpr/slice | solution.py:60
  159.0 4.5 %slice.1594 = f32[255,128]{0,1:T(8,128)S(1)} slice(f32[512,128]{0,1:T(8,128)S(1)} %bitcast.195), slice={[2:512:2], [0:128:1]} | slice | bytes 261120 | tf_op jit(solution)/shard_map/while/body/eval_jaxpr/slice | solution.py:60
  166.8 0.6 pad_maximum_fusion.126
  167.7 0.8 multiply_add_fusion.31
  168.5 0.5 slice_bitcast_fusion.6
  169.4 0.5 slice_bitcast_fusion.7
  170.3 0.8 fusion.70
  171.1 0.6 pad_add_fusion.9
  172.3 4.5 %slice.1651 = f32[255,128]{0,1:T(8,128)S(1)} slice(f32[512,128]{0,1:T(8,128)S(1)} %bitcast.197), slice={[2:512:2], [0:128:1]} | slice | bytes 261120 | tf_op jit(solution)/shard_map/while/body/eval_jaxpr/slice | solution.py:60
  176.9 4.5 %slice.1598 = f32[256,128]{0,1:T(8,128)S(1)} slice(f32[512,128]{0,1:T(8,128)S(1)} %bitcast.198), slice={[1:512:2], [0:128:1]} | slice | bytes 262144 | tf_op jit(solution)/shard_map/while/body/eval_jaxpr/slice | solution.py:60
  181.4 4.5 %slice.1596 = f32[256,128]{0,1:T(8,128)S(1)} slice(f32[512,128]{0,1:T(8,128)S(1)} %bitcast.199), slice={[0:511:2], [0:128:1]} | slice | bytes 262144 | tf_op jit(solution)/shard_map/while/body/eval_jaxpr/slice | solution.py:60
  186.6 4.5 %slice.1597 = f32[256,128]{0,1:T(8,128)S(1)} slice(f32[512,128]{0,1:T(8,128)S(1)} %bitcast.193), slice={[0:511:2], [0:128:1]} | slice | bytes 262144 | tf_op jit(solution)/shard_map/while/body/eval_jaxpr/slice | solution.py:60
  191.2 4.5 %slice.1595 = f32[256,128]{0,1:T(8,128)S(1)} slice(f32[512,128]{0,1:T(8,128)S(1)} %bitcast.194), slice={[1:512:2], [0:128:1]} | slice | bytes 262144 | tf_op jit(solution)/shard_map/while/body/eval_jaxpr/slice | solution.py:60
  195.7 4.5 %slice.1594 = f32[255,128]{0,1:T(8,128)S(1)} slice(f32[512,128]{0,1:T(8,128)S(1)} %bitcast.195), slice={[2:512:2], [0:128:1]} | slice | bytes 261120 | tf_op jit(solution)/shard_map/while/body/eval_jaxpr/slice | solution.py:60
  203.5 0.6 pad_maximum_fusion.126
  204.4 0.8 multiply_add_fusion.31
  206.1 0.5 slice_bitcast_fusion.7
  207.0 0.8 fusion.70
  207.8 0.6 pad_add_fusion.9
  209.0 4.5 %slice.1651 = f32[255,128]{0,1:T(8,128)S(1)} slice(f32[512,128]{0,1:T(8,128)S(1)} %bitcast.197), slice={[2:512:2], [0:128:1]} | slice | bytes 261120 | tf_op jit(solution)/shard_map/while/body/eval_jaxpr/slice | solution.py:60
  213.6 4.5 %slice.1598 = f32[256,128]{0,1:T(8,128)S(1)} slice(f32[512,128]{0,1:T(8,128)S(1)} %bitcast.198), slice={[1:512:2], [0:128:1]} | slice | bytes 262144 | tf_op jit(solution)/shard_map/while/body/eval_jaxpr/slice | solution.py:60
  218.1 4.5 %slice.1596 = f32[256,128]{0,1:T(8,128)S(1)} slice(f32[512,128]{0,1:T(8,128)S(1)} %bitcast.199), slice={[0:511:2], [0:128:1]} | slice | bytes 262144 | tf_op jit(solution)/shard_map/while/body/eval_jaxpr/slice | solution.py:60
  223.3 4.5 %slice.1597 = f32[256,128]{0,1:T(8,128)S(1)} slice(f32[512,128]{0,1:T(8,128)S(1)} %bitcast.193), slice={[0:511:2], [0:128:1]} | slice | bytes 262144 | tf_op jit(solution)/shard_map/while/body/eval_jaxpr/slice | solution.py:60
  227.8 4.5 %slice.1595 = f32[256,128]{0,1:T(8,128)S(1)} slice(f32[512,128]{0,1:T(8,128)S(1)} %bitcast.194), slice={[1:512:2], [0:128:1]} | slice | bytes 262144 | tf_op jit(solution)/shard_map/while/body/eval_jaxpr/slice | solution.py:60
  232.3 4.5 %slice.1594 = f32[255,128]{0,1:T(8,128)S(1)} slice(f32[512,128]{0,1:T(8,128)S(1)} %bitcast.195), slice={[2:512:2], [0:128:1]} | slice | bytes 261120 | tf_op jit(solution)/shard_map/while/body/eval_jaxpr/slice | solution.py:60
  240.2 0.6 pad_maximum_fusion.126
  241.1 0.8 multiply_add_fusion.31
  242.8 0.5 slice_bitcast_fusion.7
  243.7 0.8 fusion.70
  244.7 11.1 %all_to_all.35 = bf16[16,128,32]{1,2,0:T(8,128)(2,1)S(1)} all-to-all(bf16[16,128,32]{1,2,0:T(8,128)(2,1)S(1)} %copy.44), channel_id=1, replica_groups=mesh['sp'=16,'dp'=8] {'sp'}, dimensions={0} | all-to-all | bytes 262144 | tf_op jit(solution)/shard_map/all_to_all | solution.py:124
  255.8 2.5 fusion.11
  258.3 3.2 %fusion.13 = bf16[1,128,2048]{2,1,0:T(8,128)(2,1)} fusion(f32[128,2048]{1,0:T(8,128)S(1)} %fusion.11, bf16[128,512]{0,1:T(8,128)(2,1)S(1)} %bitcast.207, bf16[2048,1536]{1,0:T(8,128)(2,1)} %all-gather.2.cloned.1.call-done), kind=kOutput, calls=%fused_computation.131 | convolution fusion | flops 268959744 | bytes 3801088 | tf_op jit(solution)/shard_map/dot_general | solution.py:125
  (888 shorter events, 20.9 us)
Async XLA Ops:
  6.5 74.7 %copy-start = (bf16[1,128,2048]{2,1,0:T(8,128)(2,1)S(1)}, bf16[1,128,2048]{2,1,0:T(8,128)(2,1)}, u32[]{:S(2)}) copy-start(bf16[1,128,2048]{2,1,0:T(8,128)(2,1)} %param.14) | copy-start | bytes 1572868
  6.5 74.7 %all-gather.2.cloned.1.call-start = ((), (), s32[]{:S(2)}) async-start(), calls=%async_computation.2 | async-start | bytes 6340608 | tf_op jit(solution)/shard_map/all_gather | solution.py:12
  9.6 79.9 %copy-start.1 = (f32[2,64]{1,0:T(2,128)}, f32[2,64]{1,0:T(2,128)S(1)}, u32[]{:S(2)}) copy-start(f32[2,64]{1,0:T(2,128)S(1)} %get-tuple-element.1126) | copy-start | bytes 1540
  9.6 79.9 %copy-start.2 = (f32[2,64]{1,0:T(2,128)}, f32[2,64]{1,0:T(2,128)S(1)}, u32[]{:S(2)}) copy-start(f32[2,64]{1,0:T(2,128)S(1)} %get-tuple-element.1125) | copy-start | bytes 1540
  84.2 12.4 %all-to-all-start = ((bf16[128,16,32]{0,2,1:T(8,128)(2,1)}), bf16[128,16,32]{0,2,1:T(8,128)(2,1)S(1)}, u32[]{:S(2)}, u32[]{:S(2)}) async-start(bf16[128,16,32]{0,2,1:T(8,128)(2,1)} %bitcast.33), calls=%async_computation | async-start | bytes 262144 | tf_op jit(solution)/shard_map/all_to_all | solution.py:120
Sparse Core Ops, SparseCore 0:
  10.4 70.7 all-gather.1
where the time goes:
time: 269 us; the launch traced here: 268 us
  local copies, waits for them, and re-layouts  127 us (47%)
  waiting for transfers between devices  74.2 us (28%)
  other arithmetic  19.4 us (7%)
  between operations  13.5 us (5%)
  matrix products  13.3 us (5%)
  blocking collectives  11.1 us (4%)
  loops' own time  5.28 us (2%)
  starting transfers between devices  4.36 us (2%)
    slice x250, local copies, waits for them, and re-layouts, block_scan(): lax.associative_scan(combine, (are, aim, drive_re, drive_im), axis=0)  112 us
    all_gather x1, waiting for transfers between devices, rows_first(): out = lax.all_gather(both, axis, axis=0, tiled=True)  69.2 us
    all_to_all x1, blocking collectives, shards(): lax.all_to_all(mixer_local, 'sp', split_axis=0, concat_axis=1, tiled=True)  11.1 us
  transfers between devices with their start and end apart: 2, of which 2 were waited for; matrix products, arithmetic and copies ran while one was open for 3% of the time, Pallas kernels for 0%

commit v1 on v0

--- a/solution.py
+++ b/solution.py
@@ -5,11 +5,18 @@
 from jax.sharding import PartitionSpec as P
 
 
+def push_the_slots(body, shard_axis):
+    r2 = tuple((body for _ in range(lax.axis_size(shard_axis))))
+    a_next = jnp.stack(r2, axis=0)
+    x_next = lax.all_to_all(a_next, shard_axis, split_axis=0, concat_axis=0)
+    return jnp.concatenate(x_next, axis=0)
+
+
 def rows_first(arrays, axis, dims):
     turned = [jnp.moveaxis(a, dim, 0) for a, dim in zip(arrays, dims)]
     widths = [t[0].size for t in turned]
     both = jnp.concatenate([t.reshape(-1, w) for t, w in zip(turned, widths)], axis=1)
-    out = lax.all_gather(both, axis, axis=0, tiled=True)
+    out = push_the_slots(both, axis)
     tiles = jnp.split(out, [sum(widths[:k]) for k in range(1, len(widths))], axis=1)
     return tuple(
         (

time: 269 us -> 393 us (1.46)
  other arithmetic: 19.4 us -> 123 us
  local copies, waits for them, and re-layouts: 127 us -> 141 us
  between operations: 13.5 us -> 0.09 us
  starting transfers between devices: 4.36 us -> 15.6 us
  matrix products: 13.3 us -> 21.9 us
  waiting for transfers between devices: 74.2 us -> 69.6 us
    all_gather x1 -> x0, waiting for transfers between devices: 69.2 us -> none  [rows_first(): out = lax.all_gather(both, axis, axis=0, tiled=True)]
    all_to_all x0 -> x1, waiting for transfers between devices: none -> 68 us  [push_the_slots(): x_next = lax.all_to_all(a_next, shard_axis, split_axis=0, concat_axis=0)]
    concatenate x128, other arithmetic: 3.75 us -> 42.4 us  [block_scan(): lax.associative_scan(combine, (are, aim, drive_re, drive_im), axis=0)]
    add x44, other arithmetic: 0.96 us -> 31.3 us  [combine(): rre * lbim + rim * lbre + rbim]
    add x26, other arithmetic: 0.38 us -> 18.1 us  [combine(): rre * lim + rim * lre]
    all_to_all x0 -> x1, starting transfers between devices: none -> 11.6 us  [push_the_slots(): x_next = lax.all_to_all(a_next, shard_axis, split_axis=0, concat_axis=0)]
    add x16, other arithmetic: 0.15 us -> 10.4 us  [combine(): rre * lbre - rim * lbim + rbre]
where the time goes in v1:
time: 393 us; the launch traced here: 389 us
  local copies, waits for them, and re-layouts  141 us (36%)
  other arithmetic  123 us (31%)
  waiting for transfers between devices  69.6 us (18%)
  matrix products  21.9 us (6%)
  starting transfers between devices  15.6 us (4%)
  blocking collectives  13.4 us (3%)
    slice x250, local copies, waits for them, and re-layouts, block_scan(): lax.associative_scan(combine, (are, aim, drive_re, drive_im), axis=0)  113 us
    all_to_all x1, waiting for transfers between devices, push_the_slots(): x_next = lax.all_to_all(a_next, shard_axis, split_axis=0, concat_axis=0)  68 us
    concatenate x128, other arithmetic, block_scan(): lax.associative_scan(combine, (are, aim, drive_re, drive_im), axis=0)  42.4 us
    add x44, other arithmetic, combine(): rre * lbim + rim * lbre + rbim  31.3 us
    add x26, other arithmetic, combine(): rre * lim + rim * lre  18.1 us
    all_to_all x1, blocking collectives, shards(): lax.all_to_all(mixer_local, 'sp', split_axis=0, concat_axis=1, tiled=True)  13.4 us
    all_to_all x1, starting transfers between devices, push_the_slots(): x_next = lax.all_to_all(a_next, shard_axis, split_axis=0, concat_axis=0)  11.6 us
    add x16, other arithmetic, combine(): rre * lbre - rim * lbim + rbre  10.4 us
  transfers between devices with their start and end apart: 2, of which 2 were waited for; matrix products, arithmetic and copies ran while one was open for 3% of the time, Pallas kernels for 0%

profile of v1, /device:TPU:0, one launch (start us, length us, event | category | flops | bytes accessed | tf_op | source)
XLA Modules:
  0.0 388.8 jit_solution(3769375787160031090)
XLA Ops:
  0.0 0.8 pad_maximum_fusion.32
  0.8 3.4 stack.2
  4.2 11.6 %all-to-all-start = ((bf16[128,16,1536]{2,1,0:T(8,128)(2,1)}), bf16[128,16,1536]{2,1,0:T(8,128)(2,1)}, u32[]{:S(2)}, u32[]{:S(2)}) async-start(bf16[128,16,1536]{2,1,0:T(8,128)(2,1)} %stack.2), calls=%async_computation | async-start | bytes 12582912 | tf_op jit(solution)/shard_map/all_to_all | solution.py:11
  16.0 0.8 multiply_subtract_fusion.10
  16.8 0.8 add_divide_fusion
  20.2 1.3 add_multiply_fusion.9
  21.5 1.3 multiply_add_fusion.9
  22.9 68.0 %all-to-all-done = bf16[128,16,1536]{2,1,0:T(8,128)(2,1)} async-done(((bf16[128,16,1536]{2,1,0:T(8,128)(2,1)}), bf16[128,16,1536]{2,1,0:T(8,128)(2,1)}, u32[]{:S(2)}, u32[]{:S(2)}) %all-to-all-start) | async-done | bytes 6291488 | tf_op jit(solution)/shard_map/all_to_all | solution.py:11
  90.9 3.0 fusion.18
  93.9 4.0 %all-to-all-start.1 = ((bf16[128,16,32]{0,2,1:T(8,128)(2,1)}), bf16[128,16,32]{0,2,1:T(8,128)(2,1)S(1)}, u32[]{:S(2)}, u32[]{:S(2)}) async-start(bf16[128,16,32]{0,2,1:T(8,128)(2,1)} %bitcast.34), calls=%async_computation.1 | async-start | bytes 262144 | tf_op jit(solution)/shard_map/all_to_all | solution.py:127
  97.9 1.2 multiply_subtract_fusion.20
  101.6 1.3 dynamic_slice.38
  102.9 1.3 constant_dynamic-slice_fusion.1
  104.2 1.6 all-to-all-done.1
  107.8 260.8 %while.18 = (s32[]{:T(128)}, f32[128]{0:T(128)}, f32[128]{0:T(128)}, bf16[4,512,32]{1,2,0:T(8,128)(2,1)}, bf16[4,512,32]{1,2,0:T(8,128)(2,1)}, /*index=5*/f32[2,...) while((s32[]{:T(128)}, f32[128]{0:T(128)}, ...), condition=%wide.wide.region_1.2_spmd, body=%wide.wide.region_0.1_spmd.sunk | while | flops 53527552 | bytes 26573368 | solution.py:91
  108.8 4.5 %slice.1595 = f32[256,128]{0,1:T(8,128)S(1)} slice(f32[512,128]{0,1:T(8,128)S(1)} %bitcast.193), slice={[1:512:2], [0:128:1]} | slice | bytes 262144 | tf_op jit(solution)/shard_map/while/body/eval_jaxpr/slice | solution.py:67
  113.4 1.0 fusion.68
  114.5 4.5 %slice.1596 = f32[256,128]{0,1:T(8,128)S(1)} slice(f32[512,128]{0,1:T(8,128)S(1)} %bitcast.197), slice={[0:511:2], [0:128:1]} | slice | bytes 262144 | tf_op jit(solution)/shard_map/while/body/eval_jaxpr/slice | solution.py:67
  119.1 4.5 %slice.1597 = f32[256,128]{0,1:T(8,128)S(1)} slice(f32[512,128]{0,1:T(8,128)S(1)} %bitcast.194), slice={[0:511:2], [0:128:1]} | slice | bytes 262144 | tf_op jit(solution)/shard_map/while/body/eval_jaxpr/slice | solution.py:67
  123.7 4.5 %slice.1598 = f32[256,128]{0,1:T(8,128)S(1)} slice(f32[512,128]{0,1:T(8,128)S(1)} %bitcast.198), slice={[1:512:2], [0:128:1]} | slice | bytes 262144 | tf_op jit(solution)/shard_map/while/body/eval_jaxpr/slice | solution.py:67
  156.1 4.5 %slice.1594 = f32[255,128]{0,1:T(8,128)S(1)} slice(f32[512,128]{0,1:T(8,128)S(1)} %bitcast.195), slice={[2:512:2], [0:128:1]} | slice | bytes 261120 | tf_op jit(solution)/shard_map/while/body/eval_jaxpr/slice | solution.py:67
  160.7 4.5 %slice.1651 = f32[255,128]{0,1:T(8,128)S(1)} slice(f32[512,128]{0,1:T(8,128)S(1)} %bitcast.199), slice={[2:512:2], [0:128:1]} | slice | bytes 261120 | tf_op jit(solution)/shard_map/while/body/eval_jaxpr/slice | solution.py:67
  165.9 1.0 add_add_fusion.47
  168.3 1.0 fusion.69
  169.4 1.0 convolution_subtract_fusion.3
  170.4 1.5 fusion.70
  174.0 4.5 %slice.1595 = f32[256,128]{0,1:T(8,128)S(1)} slice(f32[512,128]{0,1:T(8,128)S(1)} %bitcast.193), slice={[1:512:2], [0:128:1]} | slice | bytes 262144 | tf_op jit(solution)/shard_map/while/body/eval_jaxpr/slice | solution.py:67
  178.6 1.0 fusion.68
  179.7 4.5 %slice.1596 = f32[256,128]{0,1:T(8,128)S(1)} slice(f32[512,128]{0,1:T(8,128)S(1)} %bitcast.197), slice={[0:511:2], [0:128:1]} | slice | bytes 262144 | tf_op jit(solution)/shard_map/while/body/eval_jaxpr/slice | solution.py:67
  184.3 4.5 %slice.1597 = f32[256,128]{0,1:T(8,128)S(1)} slice(f32[512,128]{0,1:T(8,128)S(1)} %bitcast.194), slice={[0:511:2], [0:128:1]} | slice | bytes 262144 | tf_op jit(solution)/shard_map/while/body/eval_jaxpr/slice | solution.py:67
  188.9 4.5 %slice.1598 = f32[256,128]{0,1:T(8,128)S(1)} slice(f32[512,128]{0,1:T(8,128)S(1)} %bitcast.198), slice={[1:512:2], [0:128:1]} | slice | bytes 262144 | tf_op jit(solution)/shard_map/while/body/eval_jaxpr/slice | solution.py:67
  221.3 4.5 %slice.1594 = f32[255,128]{0,1:T(8,128)S(1)} slice(f32[512,128]{0,1:T(8,128)S(1)} %bitcast.195), slice={[2:512:2], [0:128:1]} | slice | bytes 261120 | tf_op jit(solution)/shard_map/while/body/eval_jaxpr/slice | solution.py:67
  225.9 4.5 %slice.1651 = f32[255,128]{0,1:T(8,128)S(1)} slice(f32[512,128]{0,1:T(8,128)S(1)} %bitcast.199), slice={[2:512:2], [0:128:1]} | slice | bytes 261120 | tf_op jit(solution)/shard_map/while/body/eval_jaxpr/slice | solution.py:67
  231.1 1.0 add_add_fusion.47
  232.5 0.8 multiply_add_fusion.31
  233.5 1.0 fusion.69
  234.6 1.0 convolution_subtract_fusion.3
  235.6 1.5 fusion.70
  239.2 4.5 %slice.1595 = f32[256,128]{0,1:T(8,128)S(1)} slice(f32[512,128]{0,1:T(8,128)S(1)} %bitcast.193), slice={[1:512:2], [0:128:1]} | slice | bytes 262144 | tf_op jit(solution)/shard_map/while/body/eval_jaxpr/slice | solution.py:67
  243.8 1.0 fusion.68
  244.9 4.5 %slice.1596 = f32[256,128]{0,1:T(8,128)S(1)} slice(f32[512,128]{0,1:T(8,128)S(1)} %bitcast.197), slice={[0:511:2], [0:128:1]} | slice | bytes 262144 | tf_op jit(solution)/shard_map/while/body/eval_jaxpr/slice | solution.py:67
  249.5 4.5 %slice.1597 = f32[256,128]{0,1:T(8,128)S(1)} slice(f32[512,128]{0,1:T(8,128)S(1)} %bitcast.194), slice={[0:511:2], [0:128:1]} | slice | bytes 262144 | tf_op jit(solution)/shard_map/while/body/eval_jaxpr/slice | solution.py:67
  254.1 4.5 %slice.1598 = f32[256,128]{0,1:T(8,128)S(1)} slice(f32[512,128]{0,1:T(8,128)S(1)} %bitcast.198), slice={[1:512:2], [0:128:1]} | slice | bytes 262144 | tf_op jit(solution)/shard_map/while/body/eval_jaxpr/slice | solution.py:67
  286.5 4.5 %slice.1594 = f32[255,128]{0,1:T(8,128)S(1)} slice(f32[512,128]{0,1:T(8,128)S(1)} %bitcast.195), slice={[2:512:2], [0:128:1]} | slice | bytes 261120 | tf_op jit(solution)/shard_map/while/body/eval_jaxpr/slice | solution.py:67
  291.1 4.5 %slice.1651 = f32[255,128]{0,1:T(8,128)S(1)} slice(f32[512,128]{0,1:T(8,128)S(1)} %bitcast.199), slice={[2:512:2], [0:128:1]} | slice | bytes 261120 | tf_op jit(solution)/shard_map/while/body/eval_jaxpr/slice | solution.py:67
  296.3 1.0 add_add_fusion.47
  298.7 1.0 fusion.69
  299.8 1.0 convolution_subtract_fusion.3
  300.8 1.5 fusion.70
  304.4 4.5 %slice.1595 = f32[256,128]{0,1:T(8,128)S(1)} slice(f32[512,128]{0,1:T(8,128)S(1)} %bitcast.193), slice={[1:512:2], [0:128:1]} | slice | bytes 262144 | tf_op jit(solution)/shard_map/while/body/eval_jaxpr/slice | solution.py:67
  309.0 1.0 fusion.68
  310.1 4.5 %slice.1596 = f32[256,128]{0,1:T(8,128)S(1)} slice(f32[512,128]{0,1:T(8,128)S(1)} %bitcast.197), slice={[0:511:2], [0:128:1]} | slice | bytes 262144 | tf_op jit(solution)/shard_map/while/body/eval_jaxpr/slice | solution.py:67
  314.7 4.5 %slice.1597 = f32[256,128]{0,1:T(8,128)S(1)} slice(f32[512,128]{0,1:T(8,128)S(1)} %bitcast.194), slice={[0:511:2], [0:128:1]} | slice | bytes 262144 | tf_op jit(solution)/shard_map/while/body/eval_jaxpr/slice | solution.py:67
  319.3 4.5 %slice.1598 = f32[256,128]{0,1:T(8,128)S(1)} slice(f32[512,128]{0,1:T(8,128)S(1)} %bitcast.198), slice={[1:512:2], [0:128:1]} | slice | bytes 262144 | tf_op jit(solution)/shard_map/while/body/eval_jaxpr/slice | solution.py:67
  351.7 4.5 %slice.1594 = f32[255,128]{0,1:T(8,128)S(1)} slice(f32[512,128]{0,1:T(8,128)S(1)} %bitcast.195), slice={[2:512:2], [0:128:1]} | slice | bytes 261120 | tf_op jit(solution)/shard_map/while/body/eval_jaxpr/slice | solution.py:67
  356.3 4.5 %slice.1651 = f32[255,128]{0,1:T(8,128)S(1)} slice(f32[512,128]{0,1:T(8,128)S(1)} %bitcast.199), slice={[2:512:2], [0:128:1]} | slice | bytes 261120 | tf_op jit(solution)/shard_map/while/body/eval_jaxpr/slice | solution.py:67
  361.5 1.0 add_add_fusion.47
  363.9 1.0 fusion.69
  365.0 1.0 convolution_subtract_fusion.3
  366.0 1.5 fusion.70
  368.5 1.0 copy.43
  369.7 13.4 %all_to_all.40 = bf16[16,128,32]{1,2,0:T(8,128)(2,1)S(1)} all-to-all(bf16[16,128,32]{1,2,0:T(8,128)(2,1)S(1)} %copy.44), channel_id=1, replica_groups=mesh['sp'=16,'dp'=8] {'sp'}, dimensions={0} | all-to-all | bytes 262144 | tf_op jit(solution)/shard_map/all_to_all | solution.py:131
  383.1 2.5 fusion.11
  385.5 3.2 fusion.13
  (890 shorter events, 133.9 us)
Async XLA Ops:
  0.0 90.9 %copy-start = (bf16[1,128,2048]{2,1,0:T(8,128)(2,1)S(1)}, bf16[1,128,2048]{2,1,0:T(8,128)(2,1)}, u32[]{:S(2)}) copy-start(bf16[1,128,2048]{2,1,0:T(8,128)(2,1)} %param.14) | copy-start | bytes 1572868
  4.2 11.7 %copy-start.3 = (f32[32]{0:T(128)S(1)}, f32[32]{0:T(128)}, u32[]{:S(2)}) copy-start(f32[32]{0:T(128)} %param.18) | copy-start | bytes 388
  4.2 86.7 %all-to-all-start = ((bf16[128,16,1536]{2,1,0:T(8,128)(2,1)}), bf16[128,16,1536]{2,1,0:T(8,128)(2,1)}, u32[]{:S(2)}, u32[]{:S(2)}) async-start(bf16[128,16,1536]{2,1,0:T(8,128)(2,1)} %stack.2), calls=%async_computation | async-start | bytes 12582912 | tf_op jit(solution)/shard_map/all_to_all | solution.py:11
  16.8 89.1 %copy-start.1 = (f32[2,64]{1,0:T(2,128)}, f32[2,64]{1,0:T(2,128)S(1)}, u32[]{:S(2)}) copy-start(f32[2,64]{1,0:T(2,128)S(1)} %get-tuple-element.1126) | copy-start | bytes 1540
  16.8 89.1 %copy-start.2 = (f32[2,64]{1,0:T(2,128)}, f32[2,64]{1,0:T(2,128)S(1)}, u32[]{:S(2)}) copy-start(f32[2,64]{1,0:T(2,128)S(1)} %get-tuple-element.1125) | copy-start | bytes 1540
  93.9 11.9 %all-to-all-start.1 = ((bf16[128,16,32]{0,2,1:T(8,128)(2,1)}), bf16[128,16,32]{0,2,1:T(8,128)(2,1)S(1)}, u32[]{:S(2)}, u32[]{:S(2)}) async-start(bf16[128,16,32]{0,2,1:T(8,128)(2,1)} %bitcast.34), calls=%async_computation.1 | async-start | bytes 262144 | tf_op jit(solution)/shard_map/all_to_all | solution.py:127
